TPU v7x, 512 devices: a whole 4x8x8 slice. The times are simulated.
512 devices in a mesh: sp: 32 (over z, x), tp: 16 (over y, core).
Axes of the slice: x: 4, y: 8, z: 8, core: 2. Of those that a mesh axis runs over, the one named last changes fastest.
Arguments:
- pool_input: bfloat16 [8192, 1024], P('sp', 'tp'), may hold values from -6 to 6
- pool_weight: bfloat16 [16, 64, 64], P('tp'), may hold values from -0.75 to 0.75
- pool_gain: bfloat16 [1024], P('tp'), may hold values from 0.099609375 to 1.8984375
- out_weight: bfloat16 [1024, 2048], P(None, 'tp'), may hold values from -0.1875 to 0.1875
- resid: bfloat16 [8192, 2048], P('sp', 'tp'), may hold values from -90 to 90
- norm_gain: bfloat16 [2048], P('tp'), may hold values from 0.099609375 to 1.8984375
- routes: int32 [8192, 2], P('sp'), may hold values from 0 to 31, all different within a row; in each aligned block of 256 rows (0 to 255, 256 to 511, ...) at most 32 rows name the same one
- route_weight: float32 [8192, 2], P('sp'), may hold values from 0.2 to 1
- expert_gate: bfloat16 [32, 2048, 4096], P('sp', None, 'tp'), may hold values from -0.375 to 0.375
- expert_up: bfloat16 [32, 2048, 4096], P('sp', None, 'tp'), may hold values from -0.375 to 0.375
- expert_down: bfloat16 [32, 4096, 2048], P('sp', 'tp'), may hold values from -0.0234375 to 0.0234375
Outputs:
- layer_out: bfloat16 [8192, 2048], P('sp', 'tp')
Inputs may be any that keep to these rules, and one draw needn't show every extreme that they name: `routes`: the 2 experts of a position differ. In each aligned block of 256 positions no expert is named by more than 32 assignments; some block reaches that bound.
All inputs are finite; a program needn't handle non-finite values.
Results may differ from a plain program's by a relative error of at most 0.0085.
Values may be sent and summed in bfloat16 or wider, within the bound.
No kernel may reach another device: no remote copies, remote signals or barrier semaphores. Data moves between devices by JAX's collectives and lax.ppermute only.
A program may use at most 64 MiB of HBM per device.

v0:
```python
import jax
import jax.numpy as jnp
from jax import lax
from jax.sharding import PartitionSpec as P

D = 2048
GSIZE = 64
REACH = 16
TOPK = 2
GATE_LIMIT = 7.0
GATE_ALPHA = 1.702
NORM_EPS = 1e-05


def from_behind(value, axis, steps):
    count = lax.axis_size(axis)
    first, last = (max(0, -steps), min(count, count - steps))
    return lax.ppermute(value, axis, [(source, source + steps) for source in range(first, last)])


def sent_to_all(value, axis):
    peers = lax.axis_size(axis)
    return lax.all_to_all(
        jnp.broadcast_to(value[None], (peers, *value.shape)), axis, 0, 0, tiled=True
    )


def taken_together(value, axis):
    everything = sent_to_all(value, axis)
    return jnp.sum(everything, axis=0)


def clamped_unit(gate_pre, up_pre):
    gate_cut = jnp.minimum(gate_pre, GATE_LIMIT)
    up_cut = jnp.clip(up_pre, -GATE_LIMIT, GATE_LIMIT)
    return (up_cut + 1.0) * gate_cut * jax.nn.sigmoid(GATE_ALPHA * gate_cut)


def window_pool(extended, width_of, position, tok_count):
    summed = jnp.zeros((tok_count, extended.shape[1]), jnp.float32)
    for offset in range(REACH):
        first_row = REACH - 1 - offset
        shifted = extended[first_row : first_row + tok_count]
        summed = summed + jnp.where(offset < width_of[None, :], shifted, 0.0)
    counted = jnp.minimum(position[:, None] + 1, width_of[None, :]).astype(jnp.float32)
    current = extended[REACH - 1 :]
    return (summed / counted - current).astype(jnp.bfloat16)


def slot_of(route_block, expert_count, capacity):
    flattened = route_block.reshape(-1)
    onehot = (flattened[:, None] == jnp.arange(expert_count, dtype=jnp.int32)[None, :]).astype(
        jnp.int32
    )
    earlier = jnp.cumsum(onehot, axis=0) - onehot
    ranked = jnp.sum(earlier * onehot, axis=1)
    return flattened * capacity + ranked


def on_device(
    pool_input,
    pool_weight,
    pool_gain,
    out_weight,
    resid,
    norm_gain,
    routes,
    route_weight,
    expert_gate,
    expert_up,
    expert_down,
):
    tok_rows, channels = pool_input.shape
    groups = pool_weight.shape[0]
    features = out_weight.shape[1]
    experts_all = lax.axis_size("sp") * expert_gate.shape[0]
    capacity = 2 * tok_rows * TOPK // experts_all
    tail_rows = pool_input[tok_rows - (REACH - 1) :]
    before = from_behind(tail_rows, "sp", 1)
    extended = jnp.concatenate([before, pool_input], axis=0).astype(jnp.float32)
    first_group = lax.axis_index("tp") * groups
    width_of = 2 ** (1 + (first_group + jnp.arange(channels, dtype=jnp.int32) // GSIZE) % 4)
    position = lax.axis_index("sp") * tok_rows + jnp.arange(tok_rows, dtype=jnp.int32)
    pooled = window_pool(extended, width_of, position, tok_rows)
    grouped = jnp.einsum(
        "tgc,gcd->tgd",
        pooled.reshape(tok_rows, groups, GSIZE),
        pool_weight,
        preferred_element_type=jnp.float32,
    )
    mixed_out = (
        (grouped * pool_gain.astype(jnp.float32).reshape(groups, GSIZE))
        .astype(jnp.bfloat16)
        .reshape(tok_rows, channels)
    )
    projected = jnp.dot(
        lax.all_gather(mixed_out, "tp", axis=1, tiled=True),
        out_weight,
        preferred_element_type=jnp.float32,
    )
    stored = lax.optimization_barrier((resid.astype(jnp.float32) + projected).astype(jnp.bfloat16))
    stream = stored.astype(jnp.float32)
    squares = taken_together(jnp.sum(stream * stream, axis=1), "tp")
    scale_row = lax.rsqrt(squares / D + NORM_EPS)
    normed_part = (stream * scale_row[:, None] * norm_gain.astype(jnp.float32)).astype(jnp.bfloat16)
    slot_index = slot_of(routes, experts_all, capacity)
    token_ids = jnp.repeat(jnp.arange(tok_rows, dtype=jnp.int32), TOPK)
    slot_token = (
        jnp.full((experts_all * capacity,), tok_rows, jnp.int32).at[slot_index].set(token_ids)
    )
    sent_rows = jnp.take(normed_part, slot_token, axis=0, mode="fill", fill_value=0).reshape(
        experts_all, capacity, features
    )
    gathered = lax.all_gather(
        lax.all_to_all(sent_rows, "sp", split_axis=0, concat_axis=0, tiled=True),
        "tp",
        axis=2,
        tiled=True,
    )
    sources = gathered.shape[0]
    slot_count = gathered.shape[1]
    flattened = gathered.reshape(sources * slot_count, gathered.shape[2])
    gate_pre = jnp.dot(flattened, expert_gate[0], preferred_element_type=jnp.float32)
    up_pre = jnp.dot(flattened, expert_up[0], preferred_element_type=jnp.float32)
    hidden = clamped_unit(gate_pre, up_pre).astype(jnp.bfloat16)
    down_piece = expert_down[0]
    summed = lax.psum_scatter(
        lax.dot_general(
            down_piece, hidden, (((0,), (1,)), ((), ())), preferred_element_type=jnp.float32
        ).astype(jnp.bfloat16),
        "tp",
        scatter_dimension=0,
        tiled=True,
    ).astype(jnp.float32)
    result = summed.astype(jnp.bfloat16).reshape(summed.shape[0], sources, slot_count)
    returned = lax.all_to_all(result, "sp", split_axis=1, concat_axis=1, tiled=True)
    flat_back = returned.reshape(returned.shape[0], experts_all * capacity)
    picked = (
        jnp.take(flat_back, slot_index, axis=1)
        .astype(jnp.float32)
        .reshape(flat_back.shape[0], tok_rows, TOPK)
    )
    combined = jnp.sum(picked * route_weight[None, :, :], axis=2)
    return (stream + combined.T).astype(jnp.bfloat16)


def solution(mesh):
    in_specs = (
        P("sp", "tp"),
        P("tp", None, None),
        P("tp"),
        P(None, "tp"),
        P("sp", "tp"),
        P("tp"),
        P("sp", None),
        P("sp", None),
        P("sp", None, "tp"),
        P("sp", None, "tp"),
        P("sp", "tp", None),
    )
    out_specs = P("sp", "tp")
    return jax.shard_map(
        on_device, mesh=mesh, in_specs=in_specs, out_specs=out_specs, check_vma=False
    )
```

profile of v0, /device:TPU:25, one launch (start us, length us, event | category | flops | bytes accessed | tf_op | source)
XLA Modules:
  0.0 242.8 jit_solution(6143387055872761771)
XLA Ops:
  6.5 0.9 slice.58
  7.4 3.1 %collective-permute-start = (bf16[15,64]{0,1:T(8,128)(2,1)S(1)}, bf16[15,64]{0,1:T(8,128)(2,1)S(1)}, u32[]{:S(2)}, u32[]{:S(2)}) collective-permute-start(bf16[15,64]{0,1:T(8,128)(2,1)S(1)} %slice.58), channel_id=1, source_target_pairs={{0,16},{16,32},{32,48},{48,64},{64,80},{80,96},{96,112},{112,128},... | collective-permute-start | bytes 5768 | tf_op jit(solution)/shard_map/ppermute | solution.py:18
  10.8 0.8 copy.35
  11.9 0.7 broadcast_multiply_fusion
  12.6 1.2 reduce-window.6
  14.6 2.4 %scatter_custom_fusion = s32[1024]{0:T(1024)S(1)} fusion(s32[512]{0:T(512)S(1)} %bitcast.68, s32[512]{0:T(512)S(1)} %reshape.263, s32[]{:T(128)} %constant.149.clone.1), kind=kCustom, calls=%fused_computation.92 | custom fusion | bytes 4100 | tf_op jit(solution)/shard_map/scatter | solution.py:109
  17.8 0.8 maximum_convert_fusion
  18.6 1.3 fusion.7
  20.0 17.9 %all-gather = bf16[256,1,1024]{0,2,1:T(8,128)(2,1)S(1)} all-gather(bf16[256,1,64]{0,2,1:T(8,128)(2,1)S(1)} %fusion.7), channel_id=2, replica_groups=mesh['sp'=32,'tp'=16] {'tp'}, dimensions={2}, use_global_device_ids=true | all-gather | bytes 557056 | tf_op jit(solution)/shard_map/all_gather | solution.py:97
  37.9 1.3 fusion.4
  39.9 6.2 %all-to-all-start = ((f32[16,1,256]{2,1,0:T(1,128)}), f32[16,1,256]{2,1,0:T(1,128)S(1)}, u32[]{:S(2)}, u32[]{:S(2)}) async-start(f32[16,1,256]{2,1,0:T(1,128)} %broadcast_in_dim.187), calls=%async_computation | async-start | bytes 32768 | tf_op jit(solution)/shard_map/all_to_all | solution.py:23
  46.3 4.4 %all-to-all-done = f32[16,1,256]{2,1,0:T(1,128)S(1)} async-done(((f32[16,1,256]{2,1,0:T(1,128)}), f32[16,1,256]{2,1,0:T(1,128)S(1)}, u32[]{:S(2)}, u32[]{:S(2)}) %all-to-all-start) | async-done | bytes 16416 | tf_op jit(solution)/shard_map/all_to_all | solution.py:23
  50.8 3.2 %gather_fusion = bf16[1024,128]{1,0:T(8,128)(2,1)S(1)} fusion(bf16[256,128]{1,0:T(8,128)(2,1)S(1)} %fusion.24, s32[1024]{0:T(1024)S(1)} %fusion.50), kind=kCustom, calls=%fused_computation | custom fusion | bytes 528384 | tf_op jit(solution)/shard_map/jit(_take)/gather | solution.py:111
  54.2 24.2 %all_to_all.16 = bf16[32,32,128]{2,1,0:T(8,128)(2,1)} all-to-all(bf16[32,32,128]{2,1,0:T(8,128)(2,1)S(1)} %broadcast_select_fusion), channel_id=1, replica_groups=mesh['sp'=32,'tp'=16] {'sp'}, dimensions={0} | all-to-all | bytes 524288 | tf_op jit(solution)/shard_map/all_to_all | solution.py:115
  78.5 45.3 %all-gather.3.cloned.1.call-done = bf16[32,32,2048]{2,1,0:T(8,128)(2,1)} async-done(((bf16[32,32,128]{2,1,0:T(8,128)(2,1)}), bf16[32,32,2048]{2,1,0:T(8,128)(2,1)}) %all-gather.3.cloned.1.call-update) | async-done | bytes 4194320 | tf_op jit(solution)/shard_map/all_gather | solution.py:114
  123.7 4.5 %convolution_minimum_fusion = f32[1024,256]{1,0:T(8,128)} fusion(bf16[1024,2048]{1,0:T(8,128)(2,1)} %bitcast.70, bf16[1,2048,256]{2,1,0:T(8,128)(2,1)S(1)} %copy-done.3), kind=kOutput, calls=%fused_computation.4 | convolution fusion | flops 1074003968 | bytes 6291456 | tf_op jit(solution)/shard_map/dot_general | solution.py:123
  128.3 8.8 %convert_bitcast_fusion = bf16[2048,1024]{0,1:T(8,128)(2,1)} fusion(f32[1024,256]{1,0:T(8,128)} %convolution_minimum_fusion, bf16[1024,2048]{1,0:T(8,128)(2,1)} %bitcast.71, bf16[1,256,2048]{2,1,0:T(8,128)(2,1)S(1)} %copy-done, bf16[1,2048,256]{2,1,0:T(8,128)(2,1)S(1)} %copy-done.4), kind=kOutput, calls=%fused_computation.3 | convolution fusion | flops 2151940096 | bytes 11534336 | tf_op jit(solution)/shard_map/dot_general | solution.py:128
  137.1 6.4 %copy.43 = bf16[2048,1024]{1,0:T(8,128)(2,1)} copy(bf16[2048,1024]{0,1:T(8,128)(2,1)} %convert_bitcast_fusion) | data formatting | bytes 8388608
  143.5 66.1 %reduce-scatter.4.cloned.1.call-done = bf16[128,1024]{1,0:T(8,128)(2,1)} async-done(((bf16[2048,1024]{1,0:T(8,128)(2,1)}), bf16[128,1024]{1,0:T(8,128)(2,1)}) %reduce-scatter.4.cloned.1.call-update) | async-done | bytes 262160
  209.6 1.8 copy.44
  211.4 9.9 %all-to-all-start.2 = ((bf16[128,32,32]{0,2,1:T(8,128)(2,1)}), bf16[128,32,32]{0,2,1:T(8,128)(2,1)S(1)}, u32[]{:S(2)}, u32[]{:S(2)}) async-start(bf16[128,32,32]{0,2,1:T(8,128)(2,1)} %bitcast.14), calls=%async_computation.2 | async-start | bytes 524288 | tf_op jit(solution)/shard_map/all_to_all | solution.py:136
  221.9 10.5 %all-to-all-done.2 = bf16[128,32,32]{0,2,1:T(8,128)(2,1)S(1)} async-done(((bf16[128,32,32]{0,2,1:T(8,128)(2,1)}), bf16[128,32,32]{0,2,1:T(8,128)(2,1)S(1)}, u32[]{:S(2)}, u32[]{:S(2)}) %all-to-all-start.2) | async-done | bytes 262176 | tf_op jit(solution)/shard_map/all_to_all | solution.py:136
  232.5 1.3 gather_fusion.1
  233.8 1.5 multiply_reduce_fusion
  (57 shorter events, 4.5 us)
Async XLA Ops:
  6.5 121.7 %copy-start = (bf16[1,256,2048]{2,1,0:T(8,128)(2,1)S(1)}, bf16[1,256,2048]{2,1,0:T(8,128)(2,1)}, u32[]{:S(2)}) copy-start(bf16[1,256,2048]{2,1,0:T(8,128)(2,1)} %param.21) | copy-start | bytes 3145732
  6.5 39.6 %copy-start.5 = (bf16[128]{0:T(256)(128)(2,1)S(1)}, bf16[128]{0:T(256)(128)(2,1)}, u32[]{:S(2)}) copy-start(bf16[128]{0:T(256)(128)(2,1)} %param.16) | copy-start | bytes 772
  7.4 10.3 %collective-permute-start = (bf16[15,64]{0,1:T(8,128)(2,1)S(1)}, bf16[15,64]{0,1:T(8,128)(2,1)S(1)}, u32[]{:S(2)}, u32[]{:S(2)}) collective-permute-start(bf16[15,64]{0,1:T(8,128)(2,1)S(1)} %slice.58), channel_id=1, source_target_pairs={{0,16},{16,32},{32,48},{48,64},{64,80},{80,96},{96,112},{112,128},... | collective-permute-start | bytes 5768 | tf_op jit(solution)/shard_map/ppermute | solution.py:18
  11.6 112.2 %copy-start.3 = (bf16[1,2048,256]{2,1,0:T(8,128)(2,1)S(1)}, bf16[1,2048,256]{2,1,0:T(8,128)(2,1)}, u32[]{:S(2)}) copy-start(bf16[1,2048,256]{2,1,0:T(8,128)(2,1)} %param.19) | copy-start | bytes 3145732
  39.9 10.7 %all-to-all-start = ((f32[16,1,256]{2,1,0:T(1,128)}), f32[16,1,256]{2,1,0:T(1,128)S(1)}, u32[]{:S(2)}, u32[]{:S(2)}) async-start(f32[16,1,256]{2,1,0:T(1,128)} %broadcast_in_dim.187), calls=%async_computation | async-start | bytes 32768 | tf_op jit(solution)/shard_map/all_to_all | solution.py:23
  46.1 77.6 %all-gather.3.cloned.1.call-start = ((), (), s32[]{:S(2)}) async-start(), calls=%async_computation.4 | async-start | bytes 4456448 | tf_op jit(solution)/shard_map/all_gather | solution.py:114
  54.2 74.1 %copy-start.4 = (bf16[1,2048,256]{2,1,0:T(8,128)(2,1)S(1)}, bf16[1,2048,256]{2,1,0:T(8,128)(2,1)}, u32[]{:S(2)}) copy-start(bf16[1,2048,256]{2,1,0:T(8,128)(2,1)} %param.20) | copy-start | bytes 3145732
  78.4 131.2 %reduce-scatter.4.cloned.1.call-start = ((), (), s32[]{:S(2)}) async-start(), calls=%async_computation.5 | async-start | bytes 4456448
  143.5 78.0 %copy-start.1 = (s32[256,2]{0,1:T(2,128)S(1)}, s32[256,2]{0,1:T(2,128)}, u32[]{:S(2)}) copy-start(s32[256,2]{0,1:T(2,128)} %param.17) | copy-start | bytes 6148
  143.5 78.2 %copy-start.2 = (f32[256,2]{0,1:T(2,128)S(1)}, f32[256,2]{0,1:T(2,128)}, u32[]{:S(2)}) copy-start(f32[256,2]{0,1:T(2,128)} %param.18) | copy-start | bytes 6148
  211.4 21.1 %all-to-all-start.2 = ((bf16[128,32,32]{0,2,1:T(8,128)(2,1)}), bf16[128,32,32]{0,2,1:T(8,128)(2,1)S(1)}, u32[]{:S(2)}, u32[]{:S(2)}) async-start(bf16[128,32,32]{0,2,1:T(8,128)(2,1)} %bitcast.14), calls=%async_computation.2 | async-start | bytes 524288 | tf_op jit(solution)/shard_map/all_to_all | solution.py:136
Sparse Core Ops, SparseCore 0:
  78.6 45.1 all-gather.2
  143.7 65.9 reduce-scatter.3
where the time goes:
time: 243 us
  waiting for transfers between devices  126 us (52%)
  blocking collectives  42.1 us (17%)
  starting transfers between devices  19.3 us (8%)
  local copies, waits for them, and re-layouts  19.1 us (8%)
  matrix products  16 us (7%)
  between operations  13.6 us (6%)
  other arithmetic  6.38 us (3%)
    unnamed x3, waiting for transfers between devices  66.1 us
    all_gather x1, waiting for transfers between devices, on_device(): lax.all_gather(lax.all_to_all(sent_rows, 'sp', split_axis=0, concat_axis=...  45.3 us
    all_to_all x1, blocking collectives, on_device(): lax.all_to_all(sent_rows, 'sp', split_axis=0, concat_axis=0, tiled=True)  24.2 us
    all_gather x1, blocking collectives, on_device(): lax.all_gather(mixed_out, 'tp', axis=1, tiled=True)  17.9 us
    all_to_all x1, waiting for transfers between devices, on_device(): lax.all_to_all(result, 'sp', split_axis=1, concat_axis=1, tiled=True)  10.5 us
    all_to_all x1, starting transfers between devices, on_device(): lax.all_to_all(result, 'sp', split_axis=1, concat_axis=1, tiled=True)  9.91 us
    unnamed x16, local copies, waits for them, and re-layouts  9.15 us
    dot_general x1, matrix products, on_device(): lax.dot_general(down_piece, hidden, (((0,), (1,)), ((), ())), preferred_e...  8.85 us
  transfers between devices with their start and end apart: 5, of which 4 were waited for; matrix products, arithmetic and copies ran while one was open for 3% of the time, Pallas kernels for 0%

commit v1 on v0

--- a/solution.py
+++ b/solution.py
@@ -111,12 +111,11 @@
     sent_rows = jnp.take(normed_part, slot_token, axis=0, mode="fill", fill_value=0).reshape(
         experts_all, capacity, features
     )
-    gathered = lax.all_gather(
-        lax.all_to_all(sent_rows, "sp", split_axis=0, concat_axis=0, tiled=True),
-        "tp",
-        axis=2,
-        tiled=True,
-    )
+    part = lax.all_to_all(sent_rows, "sp", split_axis=0, concat_axis=0, tiled=True)
+    peers_2 = lax.axis_size("tp")
+    parts = jnp.stack([part for _ in range(peers_2)])
+    parts = lax.all_to_all(parts, "tp", split_axis=0, concat_axis=0)
+    gathered = jnp.concatenate(parts, axis=2)
     sources = gathered.shape[0]
     slot_count = gathered.shape[1]
     flattened = gathered.reshape(sources * slot_count, gathered.shape[2])

time: 243 us -> 296 us (1.22)
  blocking collectives: 42.1 us -> 143 us
  waiting for transfers between devices: 126 us -> 73.9 us
  local copies, waits for them, and re-layouts: 19.1 us -> 26.7 us
  matrix products: 16 us -> 12.4 us
    all_to_all x0 -> x1, blocking collectives: none -> 101 us  [on_device(): parts = lax.all_to_all(parts, 'tp', split_axis=0, concat_axis=0)]
    all_gather x1 -> x0, waiting for transfers between devices: 45.3 us -> none  [on_device(): lax.all_gather(lax.all_to_all(sent_rows, 'sp', split_axis=0, concat_axis=...]
    unnamed x3 -> x2, waiting for transfers between devices: 66.1 us -> 59 us
    reshape x0 -> x1, local copies, waits for them, and re-layouts: none -> 4.86 us  [on_device(): gathered = jnp.concatenate(parts, axis=2)]
    dot_general x1, matrix products: 4.52 us -> 1.25 us  [on_device(): jnp.dot(flattened, expert_gate[0], preferred_element_type=jnp.float32)]
    unnamed x16 -> x18, local copies, waits for them, and re-layouts: 9.15 us -> 11.1 us
  transfers between devices with their start and end apart: 5 -> 4, of which waited for: 4 -> 3; matrix products, arithmetic and copies ran while one was open for 3% -> 3% of each run, Pallas kernels for 0% -> 0%
where the time goes in v1:
time: 296 us; the launch traced here: 295 us
  blocking collectives  143 us (48%)
  waiting for transfers between devices  73.9 us (25%)
  local copies, waits for them, and re-layouts  26.7 us (9%)
  starting transfers between devices  19.2 us (6%)
  between operations  13.7 us (5%)
  matrix products  12.4 us (4%)
  other arithmetic  6.34 us (2%)
    all_to_all x1, blocking collectives, on_device(): parts = lax.all_to_all(parts, 'tp', split_axis=0, concat_axis=0)  101 us
    unnamed x2, waiting for transfers between devices  59 us
    all_to_all x1, blocking collectives, on_device(): lax.all_to_all(sent_rows, 'sp', split_axis=0, concat_axis=0, tiled=True)  24 us
    all_gather x1, blocking collectives, on_device(): lax.all_gather(mixed_out, 'tp', axis=1, tiled=True)  17.9 us
    unnamed x18, local copies, waits for them, and re-layouts  11.1 us
    all_to_all x1, waiting for transfers between devices, on_device(): lax.all_to_all(result, 'sp', split_axis=1, concat_axis=1, tiled=True)  10.6 us
    all_to_all x1, starting transfers between devices, on_device(): lax.all_to_all(result, 'sp', split_axis=1, concat_axis=1, tiled=True)  9.88 us
    dot_general x1, matrix products, on_device(): lax.dot_general(down_piece, hidden, (((0,), (1,)), ((), ())), preferred_e...  8.53 us
  transfers between devices with their start and end apart: 4, of which 3 were waited for; matrix products, arithmetic and copies ran while one was open for 3% of the time, Pallas kernels for 0%

profile of v1, /device:TPU:25, one launch (start us, length us, event | category | flops | bytes accessed | tf_op | source)
XLA Modules:
  0.0 295.4 jit_solution(8577680851631948550)
XLA Ops:
  6.5 0.9 slice.58
  7.4 3.1 %collective-permute-start = (bf16[15,64]{0,1:T(8,128)(2,1)S(1)}, bf16[15,64]{0,1:T(8,128)(2,1)S(1)}, u32[]{:S(2)}, u32[]{:S(2)}) collective-permute-start(bf16[15,64]{0,1:T(8,128)(2,1)S(1)} %slice.58), channel_id=1, source_target_pairs={{0,16},{16,32},{32,48},{48,64},{64,80},{80,96},{96,112},{112,128},... | collective-permute-start | bytes 5768 | tf_op jit(solution)/shard_map/ppermute | solution.py:18
  12.6 1.2 reduce-window.6
  14.6 2.4 scatter_custom_fusion
  17.7 0.8 maximum_convert_fusion
  18.6 1.3 fusion.29
  19.9 17.9 %all-gather = bf16[256,1,1024]{0,2,1:T(8,128)(2,1)S(1)} all-gather(bf16[256,1,64]{0,2,1:T(8,128)(2,1)S(1)} %fusion.29), channel_id=2, replica_groups=mesh['sp'=32,'tp'=16] {'tp'}, dimensions={2}, use_global_device_ids=true | all-gather | bytes 557056 | tf_op jit(solution)/shard_map/all_gather | solution.py:97
  37.8 1.3 fusion.26
  39.9 6.2 %all-to-all-start = ((f32[16,1,256]{2,1,0:T(1,128)}), f32[16,1,256]{2,1,0:T(1,128)S(1)}, u32[]{:S(2)}, u32[]{:S(2)}) async-start(f32[16,1,256]{2,1,0:T(1,128)} %broadcast_in_dim.187), calls=%async_computation | async-start | bytes 32768 | tf_op jit(solution)/shard_map/all_to_all | solution.py:23
  46.2 4.4 %all-to-all-done = f32[16,1,256]{2,1,0:T(1,128)S(1)} async-done(((f32[16,1,256]{2,1,0:T(1,128)}), f32[16,1,256]{2,1,0:T(1,128)S(1)}, u32[]{:S(2)}, u32[]{:S(2)}) %all-to-all-start) | async-done | bytes 16416 | tf_op jit(solution)/shard_map/all_to_all | solution.py:23
  50.7 3.2 %gather_fusion = bf16[1024,128]{1,0:T(8,128)(2,1)S(1)} fusion(bf16[256,128]{1,0:T(8,128)(2,1)S(1)} %fusion.46, s32[1024]{0:T(1024)S(1)} %fusion.72), kind=kCustom, calls=%fused_computation | custom fusion | bytes 528384 | tf_op jit(solution)/shard_map/jit(_take)/gather | solution.py:111
  54.2 24.0 %all_to_all.21 = bf16[32,32,128]{2,1,0:T(8,128)(2,1)S(1)} all-to-all(bf16[32,32,128]{2,1,0:T(8,128)(2,1)S(1)} %broadcast_select_fusion), channel_id=1, replica_groups=mesh['sp'=32,'tp'=16] {'sp'}, dimensions={0} | all-to-all | bytes 524288 | tf_op jit(solution)/shard_map/all_to_all | solution.py:114
  78.9 101.3 %all_to_all.22 = bf16[16,32,32,128]{3,2,1,0:T(8,128)(2,1)S(1)} all-to-all(bf16[16,32,32,128]{3,2,1,0:T(8,128)(2,1)S(1)} %stack.2), channel_id=1, replica_groups=mesh['sp'=32,'tp'=16] {'tp'}, dimensions={0} | all-to-all | bytes 8388608 | tf_op jit(solution)/shard_map/all_to_all | solution.py:117
  180.2 4.9 %copy.45 = bf16[32,32,16,128]{3,2,1,0:T(8,128)(2,1)S(1)} copy(bf16[32,32,16,128]{3,1,0,2:T(8,128)(2,1)S(1)} %bitcast.83) | data formatting | bytes 8388608 | tf_op jit(solution)/shard_map/reshape | solution.py:118
  185.1 2.0 copy-done.1
  187.1 1.3 fusion.6
  188.3 8.5 %convert_bitcast_fusion = bf16[2048,1024]{0,1:T(8,128)(2,1)} fusion(f32[1024,256]{1,0:T(8,128)S(1)} %fusion.6, bf16[128,8,16,128]{3,2,1,0:T(8,128)(2,1)} %bitcast.86, bf16[1,256,2048]{2,1,0:T(8,128)(2,1)S(1)} %copy-done, bf16[1,2048,256]{2,1,0:T(8,128)(2,1)S(1)} %copy-done.5), kind=kOutput, calls=%fused_computation.7 | convolution fusion | flops 2151940096 | bytes 11534336 | tf_op jit(solution)/shard_map/dot_general | solution.py:127
  196.9 6.4 %copy.47 = bf16[2048,1024]{1,0:T(8,128)(2,1)} copy(bf16[2048,1024]{0,1:T(8,128)(2,1)} %convert_bitcast_fusion) | data formatting | bytes 8388608
  203.3 59.0 %reduce-scatter.4.cloned.1.call-done = bf16[128,1024]{1,0:T(8,128)(2,1)} async-done(((bf16[2048,1024]{1,0:T(8,128)(2,1)}), bf16[128,1024]{1,0:T(8,128)(2,1)}) %reduce-scatter.4.cloned.1.call-update) | async-done | bytes 262160
  262.3 1.8 copy.48
  264.0 9.9 %all-to-all-start.3 = ((bf16[128,32,32]{0,2,1:T(8,128)(2,1)}), bf16[128,32,32]{0,2,1:T(8,128)(2,1)S(1)}, u32[]{:S(2)}, u32[]{:S(2)}) async-start(bf16[128,32,32]{0,2,1:T(8,128)(2,1)} %bitcast.14), calls=%async_computation.3 | async-start | bytes 524288 | tf_op jit(solution)/shard_map/all_to_all | solution.py:135
  274.5 10.6 %all-to-all-done.3 = bf16[128,32,32]{0,2,1:T(8,128)(2,1)S(1)} async-done(((bf16[128,32,32]{0,2,1:T(8,128)(2,1)}), bf16[128,32,32]{0,2,1:T(8,128)(2,1)S(1)}, u32[]{:S(2)}, u32[]{:S(2)}) %all-to-all-start.3) | async-done | bytes 262176 | tf_op jit(solution)/shard_map/all_to_all | solution.py:135
  285.1 1.3 gather_fusion.1
  286.4 1.5 multiply_reduce_fusion
  (59 shorter events, 6.7 us)
Async XLA Ops:
  6.5 181.8 %copy-start = (bf16[1,256,2048]{2,1,0:T(8,128)(2,1)S(1)}, bf16[1,256,2048]{2,1,0:T(8,128)(2,1)}, u32[]{:S(2)}) copy-start(bf16[1,256,2048]{2,1,0:T(8,128)(2,1)} %param.21) | copy-start | bytes 3145732
  6.5 39.6 %copy-start.6 = (bf16[128]{0:T(256)(128)(2,1)S(1)}, bf16[128]{0:T(256)(128)(2,1)}, u32[]{:S(2)}) copy-start(bf16[128]{0:T(256)(128)(2,1)} %param.16) | copy-start | bytes 772
  7.4 10.3 %collective-permute-start = (bf16[15,64]{0,1:T(8,128)(2,1)S(1)}, bf16[15,64]{0,1:T(8,128)(2,1)S(1)}, u32[]{:S(2)}, u32[]{:S(2)}) collective-permute-start(bf16[15,64]{0,1:T(8,128)(2,1)S(1)} %slice.58), channel_id=1, source_target_pairs={{0,16},{16,32},{32,48},{48,64},{64,80},{80,96},{96,112},{112,128},... | collective-permute-start | bytes 5768 | tf_op jit(solution)/shard_map/ppermute | solution.py:18
  39.9 10.7 %all-to-all-start = ((f32[16,1,256]{2,1,0:T(1,128)}), f32[16,1,256]{2,1,0:T(1,128)S(1)}, u32[]{:S(2)}, u32[]{:S(2)}) async-start(f32[16,1,256]{2,1,0:T(1,128)} %broadcast_in_dim.187), calls=%async_computation | async-start | bytes 32768 | tf_op jit(solution)/shard_map/all_to_all | solution.py:23
  46.1 216.2 %reduce-scatter.4.cloned.1.call-start = ((), (), s32[]{:S(2)}) async-start(), calls=%async_computation.5 | async-start | bytes 4456448
  180.2 6.8 %copy-start.4 = (bf16[1,2048,256]{2,1,0:T(8,128)(2,1)S(1)}, bf16[1,2048,256]{2,1,0:T(8,128)(2,1)}, u32[]{:S(2)}) copy-start(bf16[1,2048,256]{2,1,0:T(8,128)(2,1)} %param.19) | copy-start | bytes 3145732
  185.1 2.0 copy-start.1
  187.1 1.3 copy-start.5
  203.3 70.9 %copy-start.2 = (s32[256,2]{0,1:T(2,128)S(1)}, s32[256,2]{0,1:T(2,128)}, u32[]{:S(2)}) copy-start(s32[256,2]{0,1:T(2,128)} %param.17) | copy-start | bytes 6148
  203.3 71.1 %copy-start.3 = (f32[256,2]{0,1:T(2,128)S(1)}, f32[256,2]{0,1:T(2,128)}, u32[]{:S(2)}) copy-start(f32[256,2]{0,1:T(2,128)} %param.18) | copy-start | bytes 6148
  264.0 21.1 %all-to-all-start.3 = ((bf16[128,32,32]{0,2,1:T(8,128)(2,1)}), bf16[128,32,32]{0,2,1:T(8,128)(2,1)S(1)}, u32[]{:S(2)}, u32[]{:S(2)}) async-start(bf16[128,32,32]{0,2,1:T(8,128)(2,1)} %bitcast.14), calls=%async_computation.3 | async-start | bytes 524288 | tf_op jit(solution)/shard_map/all_to_all | solution.py:135
Sparse Core Ops, SparseCore 0:
  203.4 58.7 reduce-scatter.3
